TPU v7x, 32 devices: a whole 2x2x4 slice. The times are simulated.
32 devices in a mesh: sp: 4 (over z), fs: 4 (over y, x), tp: 2 (over core).
Axes of the slice: x: 2, y: 2, z: 4, core: 2. Of those that a mesh axis runs over, the one named last changes fastest.
Arguments:
- tokens: bfloat16 [4, 1024, 2048], P('fs', ('sp', 'tp')), may hold values from -6 to 6
- query_weight: bfloat16 [2048, 2048], P(('sp', 'fs'), 'tp'), may hold values from -0.125 to 0.125
- forget_weight: bfloat16 [2048, 2048], P(('sp', 'fs'), 'tp'), may hold values from -0.125 to 0.125
- value_weight: bfloat16 [2048, 2048], P(('sp', 'fs'), 'tp'), may hold values from -0.125 to 0.125
- convolution_gate_weight: bfloat16 [2048, 1024], P(('sp', 'fs'), 'tp'), may hold values from -0.125 to 0.125
- convolution_multiplier_weight: bfloat16 [2048, 1024], P(('sp', 'fs'), 'tp'), may hold values from -0.125 to 0.125
- convolution_input_weight: bfloat16 [2048, 1024], P(('sp', 'fs'), 'tp'), may hold values from -0.125 to 0.125
- gate_headroom: float32 [2048], P('tp'), may hold values from 9.765625e-05 to 0.06
- added_log_rate: float32 [4, 16, 1024], P('fs', 'tp', 'sp'), may hold values from -1.6 to 0
- initial_state: float32 [4, 16, 128, 128], P('fs', 'tp'), may hold values from -0.5 to 0.5
- head_norm_gain: float32 [2048], P('tp'), may hold values from 0.1 to 1.9
- convolution_taps: float32 [3, 1024], P(None, 'tp'), may hold values from -3.5 to 3.5
- convolution_bias: float32 [1024], P('tp'), may hold values from -4 to 4
- recurrence_output_weight: bfloat16 [2048, 2048], P('tp', ('sp', 'fs')), may hold values from -0.109375 to 0.109375
- convolution_output_weight: bfloat16 [1024, 2048], P('tp', ('sp', 'fs')), may hold values from -0.109375 to 0.109375
Outputs:
- mixed: bfloat16 [4, 1024, 2048], P('fs', ('sp', 'tp'))
All inputs are finite; a program needn't handle non-finite values.
Results may differ from a plain program's by a relative error of at most 0.018.
Values may be sent and summed in bfloat16 or wider, within the bound.
A program may use at most 64 MiB of HBM per device.

v0:
```python
import jax
import jax.numpy as jnp
from jax import lax
from jax.sharding import PartitionSpec as P

DK = 128
KW = 3
BLOCK_POSITIONS = 64


def carried_in(part, axis, combine, identity):
    place = lax.axis_index(axis)
    gathered = jax.tree.map(lambda a: lax.all_gather(a, axis), part)
    state = jax.tree.map(lambda a, e: jnp.zeros_like(a) + jnp.asarray(e, a.dtype), part, identity)

    def one(hop, state):
        return combine(
            state, jax.tree.map(lambda a: lax.dynamic_index_in_dim(a, hop, 0, False), gathered)
        )

    return lax.fori_loop(0, place, one, state)


def from_behind(block, axis, distance):
    devices = range(lax.axis_size(axis))
    route = [(i - distance, i) for i in devices if i - distance in devices]
    return lax.ppermute(block, axis, route)


def to_blocks(values, number_of_heads):
    number_of_blocks = values.shape[0] // BLOCK_POSITIONS
    return jnp.transpose(
        values.reshape(number_of_blocks, BLOCK_POSITIONS, number_of_heads, DK), (2, 0, 1, 3)
    )


def within_block_recurrence(
    query_vectors, forget_logits, value_vectors, gate_headroom, extra_rates
):
    number_of_heads = extra_rates.shape[0]
    number_of_blocks = query_vectors.shape[0] // BLOCK_POSITIONS
    query_scaled = to_blocks(query_vectors.astype(jnp.float32), number_of_heads) * DK ** (-0.5)
    gated_key = to_blocks(
        gate_headroom[None, :] * jax.nn.sigmoid(-forget_logits.astype(jnp.float32)), number_of_heads
    )
    forget_log_rate = (
        jnp.log1p(-gated_key)
        + extra_rates.reshape(number_of_heads, number_of_blocks, BLOCK_POSITIONS)[..., None]
    )
    values = to_blocks(value_vectors.astype(jnp.float32), number_of_heads)
    cumulative = jnp.cumsum(forget_log_rate, axis=2)
    query_decayed = query_scaled * jnp.exp(cumulative)
    key_decayed = gated_key * jnp.exp(-cumulative)
    scores = jnp.einsum(
        "hnik,hnjk->hnij", query_decayed, key_decayed, precision=lax.Precision.HIGHEST
    )
    causal = jnp.tril(jnp.ones((BLOCK_POSITIONS, BLOCK_POSITIONS), dtype=bool))
    scores = jnp.where(causal, scores, 0.0)
    within = jnp.einsum("hnij,hnjv->hniv", scores, values, precision=lax.Precision.HIGHEST)
    final_log = cumulative[:, :, -1, :]
    contrib = jnp.einsum(
        "hnck,hncv->hnkv",
        gated_key * jnp.exp(final_log[:, :, None, :] - cumulative),
        values,
        precision=lax.Precision.HIGHEST,
    )
    decays = jnp.exp(final_log)

    def advance(current, block_pair):
        return (block_pair[0][..., None] * current + block_pair[1], current)

    empty_state = jnp.zeros((number_of_heads, DK, DK), jnp.float32)
    local_total, entering = lax.scan(
        advance, empty_state, (jnp.moveaxis(decays, 1, 0), jnp.moveaxis(contrib, 1, 0))
    )
    entering = jnp.moveaxis(entering, 0, 1)
    before = jnp.exp(jnp.cumsum(final_log, axis=1) - final_log)
    device_decay = jnp.exp(jnp.sum(final_log, axis=1))
    return (query_decayed, within, entering, before, device_decay, local_total)


def finish(query_decayed, within, entering, before, carried, head_norm_gain):
    number_of_heads = query_decayed.shape[0]
    states = entering + before[..., None] * carried[:, None]
    carried_term = jnp.einsum(
        "hnck,hnkv->hncv", query_decayed, states, precision=lax.Precision.HIGHEST
    )
    length = query_decayed.shape[1] * BLOCK_POSITIONS
    recurrence_unnormed = jnp.transpose(within + carried_term, (1, 2, 0, 3)).reshape(
        length, number_of_heads, DK
    )
    mean_square = jnp.mean(recurrence_unnormed * recurrence_unnormed, axis=-1, keepdims=True)
    rec_out = (
        recurrence_unnormed
        * lax.rsqrt(mean_square + 1e-06)
        * head_norm_gain.reshape(number_of_heads, DK)
    )
    return rec_out.reshape(length, number_of_heads * DK).astype(jnp.bfloat16)


def chain_combine(earlier_part, later_part):
    return (
        earlier_part[0] * later_part[0],
        later_part[0][..., None] * earlier_part[1] + later_part[1],
    )


def shards(
    tokens,
    query_weight,
    forget_weight,
    value_weight,
    convolution_gate_weight,
    convolution_multiplier_weight,
    convolution_input_weight,
    gate_headroom,
    added_log_rate,
    initial_state,
    head_norm_gain,
    convolution_taps,
    convolution_bias,
    recurrence_output_weight,
    convolution_output_weight,
):
    own_rows = tokens[0]
    gathered = (
        lax.all_gather(query_weight, ("sp", "fs"), axis=0, tiled=True),
        lax.all_gather(forget_weight, ("sp", "fs"), axis=0, tiled=True),
        lax.all_gather(value_weight, ("sp", "fs"), axis=0, tiled=True),
        lax.all_gather(convolution_gate_weight, ("sp", "fs"), axis=0, tiled=True),
        lax.all_gather(convolution_multiplier_weight, ("sp", "fs"), axis=0, tiled=True),
        lax.all_gather(convolution_input_weight, ("sp", "fs"), axis=0, tiled=True),
        lax.all_gather(recurrence_output_weight, ("sp", "fs"), axis=1, tiled=True),
        lax.all_gather(convolution_output_weight, ("sp", "fs"), axis=1, tiled=True),
    )
    in_weights = gathered[:6]
    out_rec = gathered[6]
    out_conv = gathered[7]
    block_rows = lax.all_gather(own_rows, "tp", axis=0, tiled=True)
    projected = jnp.concatenate(
        [
            jnp.dot(block_rows, weight, preferred_element_type=jnp.float32).astype(jnp.bfloat16)
            for weight in in_weights
        ],
        axis=1,
    )
    rec_width = query_weight.shape[1]
    conv_width = convolution_gate_weight.shape[1]
    query_vectors = projected[:, :rec_width]
    forget_logits = projected[:, rec_width : 2 * rec_width]
    value_vectors = projected[:, 2 * rec_width : 3 * rec_width]
    conv_base = 3 * rec_width
    conv_gate = projected[:, conv_base : conv_base + conv_width]
    conv_mult = projected[:, conv_base + conv_width : conv_base + 2 * conv_width]
    conv_input = projected[:, conv_base + 2 * conv_width : conv_base + 3 * conv_width]
    query_decayed, within, entering, before, device_decay, local_total = within_block_recurrence(
        query_vectors, forget_logits, value_vectors, gate_headroom, added_log_rate[0]
    )
    conv_prod = conv_mult.astype(jnp.float32) * conv_input.astype(jnp.float32)
    length = conv_prod.shape[0]
    tail_rows = conv_prod[length - (KW - 1) :]
    unit_decay = jnp.ones_like(device_decay)
    empty_state = jnp.zeros_like(local_total)
    prior_decay, prior_state = carried_in(
        (device_decay, local_total), "sp", chain_combine, (unit_decay, empty_state)
    )
    prior_rows = from_behind(tail_rows, "sp", 1)
    carried = prior_decay[..., None] * initial_state[0] + prior_state
    rec_out = finish(query_decayed, within, entering, before, carried, head_norm_gain)
    extended = jnp.concatenate([prior_rows, conv_prod], axis=0)
    conv_y = jnp.broadcast_to(convolution_bias[None, :], conv_prod.shape)
    for j in range(KW):
        conv_y = conv_y + convolution_taps[j][None, :] * extended[j : j + length]
    conv_out = (conv_gate.astype(jnp.float32) * conv_y).astype(jnp.bfloat16)
    mixed = lax.psum_scatter(
        (
            jnp.dot(rec_out, out_rec, preferred_element_type=jnp.float32)
            + jnp.dot(conv_out, out_conv, preferred_element_type=jnp.float32)
        ).astype(jnp.bfloat16),
        "tp",
        scatter_dimension=0,
        tiled=True,
    )
    return mixed[None]


def solution(mesh):
    in_specs = (
        P("fs", ("sp", "tp"), None),
        P(("sp", "fs"), "tp"),
        P(("sp", "fs"), "tp"),
        P(("sp", "fs"), "tp"),
        P(("sp", "fs"), "tp"),
        P(("sp", "fs"), "tp"),
        P(("sp", "fs"), "tp"),
        P("tp"),
        P("fs", "tp", "sp"),
        P("fs", "tp", None, None),
        P("tp"),
        P(None, "tp"),
        P("tp"),
        P("tp", ("sp", "fs")),
        P("tp", ("sp", "fs")),
    )
    out_specs = P("fs", ("sp", "tp"), None)
    return jax.shard_map(shards, mesh=mesh, in_specs=in_specs, out_specs=out_specs, check_vma=False)
```

profile of v0, /device:TPU:0, one launch (start us, length us, event | category | flops | bytes accessed | tf_op | source)
XLA Modules:
  0.0 658.4 jit_solution(4386405157501010555)
XLA Ops:
  11.5 9.2 %all-gather.30.cloned.1.call-done = bf16[1,256,2048]{2,1,0:T(8,128)(2,1)} async-done(((bf16[1,128,2048]{2,1,0:T(8,128)(2,1)}), bf16[1,256,2048]{2,1,0:T(8,128)(2,1)}) %all-gather.30.cloned.1.call-update) | async-done | bytes 1048592 | tf_op jit(solution)/shard_map/all_gather | solution.py:139
  20.7 79.6 %all-gather.14.cloned.1.call-done = bf16[2048,1024]{1,0:T(8,128)(2,1)} async-done(((bf16[128,1024]{1,0:T(8,128)(2,1)}), bf16[2048,1024]{1,0:T(8,128)(2,1)}) %all-gather.14.cloned.1.call-update) | async-done | bytes 4194320 | tf_op jit(solution)/shard_map/all_gather | solution.py:127
  100.2 3.8 fusion.17
  104.0 73.2 %all-gather.16.cloned.1.call-done = bf16[2048,1024]{1,0:T(8,128)(2,1)} async-done(((bf16[128,1024]{1,0:T(8,128)(2,1)}), bf16[2048,1024]{1,0:T(8,128)(2,1)}) %all-gather.16.cloned.1.call-update) | async-done | bytes 4194320 | tf_op jit(solution)/shard_map/all_gather | solution.py:128
  177.2 4.5 fusion.14
  181.7 72.3 %all-gather.18.cloned.1.call-done = bf16[2048,1024]{1,0:T(8,128)(2,1)} async-done(((bf16[128,1024]{1,0:T(8,128)(2,1)}), bf16[2048,1024]{1,0:T(8,128)(2,1)}) %all-gather.18.cloned.1.call-update) | async-done | bytes 4194320 | tf_op jit(solution)/shard_map/all_gather | solution.py:129
  254.1 3.5 fusion.18
  260.7 2.1 convolution_bitcast_fusion
  262.8 4.6 while.26
  270.4 45.3 %all-gather.26.cloned.1.call-done = bf16[2048,512]{1,0:T(8,128)(2,1)} async-done(((bf16[128,512]{1,0:T(8,128)(2,1)}), bf16[2048,512]{1,0:T(8,128)(2,1)}) %all-gather.26.cloned.1.call-update) | async-done | bytes 2097168 | tf_op jit(solution)/shard_map/all_gather | solution.py:132
  315.7 2.6 fusion.22
  318.3 59.2 %all-gather.24.cloned.1.call-done = bf16[2048,512]{1,0:T(8,128)(2,1)} async-done(((bf16[128,512]{1,0:T(8,128)(2,1)}), bf16[2048,512]{1,0:T(8,128)(2,1)}) %all-gather.24.cloned.1.call-update) | async-done | bytes 2097168 | tf_op jit(solution)/shard_map/all_gather | solution.py:131
  377.5 2.4 fusion.21
  380.0 3.4 collective-permute-start
  383.3 13.9 %all-gather.1 = f32[32,128]{1,0:T(8,128)S(1)} all-gather(f32[8,128]{1,0:T(8,128)S(1)} %exp.41), channel_id=3, replica_groups=mesh['sp'=4,'fs'=4,'tp'=2] {'sp'}, dimensions={0}, use_global_device_ids=true | all-gather | bytes 20480 | tf_op jit(solution)/shard_map/all_gather | solution.py:13
  398.1 2.9 convolution_select_fusion
  401.7 22.1 %all-gather.32.cloned.1.call-done = f32[32,128,128]{2,1,0:T(8,128)} async-done(((f32[8,128,128]{2,1,0:T(8,128)}), f32[32,128,128]{2,1,0:T(8,128)}) %all-gather.32.cloned.1.call-update) | async-done | bytes 2097168 | tf_op jit(solution)/shard_map/all_gather | solution.py:13
  425.0 5.1 multiply_reduce_fusion
  432.1 81.8 %all-gather.20.cloned.1.call-done = bf16[1024,2048]{1,0:T(8,128)(2,1)} async-done(((bf16[1024,128]{1,0:T(8,128)(2,1)}), bf16[1024,2048]{1,0:T(8,128)(2,1)}) %all-gather.20.cloned.1.call-update) | async-done | bytes 4194320 | tf_op jit(solution)/shard_map/all_gather | solution.py:133
  514.3 3.6 fusion.48
  517.9 57.4 %all-gather.22.cloned.1.call-done = bf16[2048,512]{1,0:T(8,128)(2,1)} async-done(((bf16[128,512]{1,0:T(8,128)(2,1)}), bf16[2048,512]{1,0:T(8,128)(2,1)}) %all-gather.22.cloned.1.call-update) | async-done | bytes 2097168 | tf_op jit(solution)/shard_map/all_gather | solution.py:130
  575.3 64.3 %all-gather.28.cloned.1.call-done = bf16[512,2048]{1,0:T(8,128)(2,1)} async-done(((bf16[512,128]{1,0:T(8,128)(2,1)}), bf16[512,2048]{1,0:T(8,128)(2,1)}) %all-gather.28.cloned.1.call-update) | async-done | bytes 2097168 | tf_op jit(solution)/shard_map/all_gather | solution.py:134
  639.7 5.5 fusion
  645.1 6.7 %reduce-scatter.2.cloned.1.call-done = bf16[128,2048]{1,0:T(8,128)(2,1)} async-done(((bf16[256,2048]{1,0:T(8,128)(2,1)}), bf16[128,2048]{1,0:T(8,128)(2,1)}) %reduce-scatter.2.cloned.1.call-update) | async-done | bytes 524304 | tf_op jit(solution)/shard_map/reduce_scatter | solution.py:175
  (86 shorter events, 20.3 us)
Async XLA Ops:
  6.5 14.1 %all-gather.30.cloned.1.call-start = ((), (), s32[]{:S(2)}) async-start(), calls=%async_computation.10 | async-start | bytes 1572864 | tf_op jit(solution)/shard_map/all_gather | solution.py:139
  7.3 93.0 %all-gather.14.cloned.1.call-start = ((), (), s32[]{:S(2)}) async-start(), calls=%async_computation.1 | async-start | bytes 4456448 | tf_op jit(solution)/shard_map/all_gather | solution.py:127
  8.0 169.2 %all-gather.16.cloned.1.call-start = ((), (), s32[]{:S(2)}) async-start(), calls=%async_computation.2 | async-start | bytes 4456448 | tf_op jit(solution)/shard_map/all_gather | solution.py:128
  8.7 245.3 %all-gather.18.cloned.1.call-start = ((), (), s32[]{:S(2)}) async-start(), calls=%async_computation.3 | async-start | bytes 4456448 | tf_op jit(solution)/shard_map/all_gather | solution.py:129
  9.3 306.4 %all-gather.26.cloned.1.call-start = ((), (), s32[]{:S(2)}) async-start(), calls=%async_computation.7 | async-start | bytes 2228224 | tf_op jit(solution)/shard_map/all_gather | solution.py:132
  9.9 367.6 %all-gather.24.cloned.1.call-start = ((), (), s32[]{:S(2)}) async-start(), calls=%async_computation.6 | async-start | bytes 2228224 | tf_op jit(solution)/shard_map/all_gather | solution.py:131
  10.5 413.3 %all-gather.32.cloned.1.call-start = ((), (), s32[]{:S(2)}) async-start(), calls=%async_computation.11 | async-start | bytes 2621440 | tf_op jit(solution)/shard_map/all_gather | solution.py:13
  11.4 165.8 %copy-start.12 = (f32[1024]{0:T(1024)S(1)}, f32[1024]{0:T(1024)}, u32[]{:S(2)}) copy-start(f32[1024]{0:T(1024)} %param.26) | copy-start | bytes 12292
  20.7 156.6 %copy-start.3 = (bf16[1,256,2048]{2,1,0:T(8,128)(2,1)S(1)}, bf16[1,256,2048]{2,1,0:T(8,128)(2,1)}, u32[]{:S(2)}) copy-start(bf16[1,256,2048]{2,1,0:T(8,128)(2,1)} %all-gather.30.cloned.1.call-done) | copy-start | bytes 3145732
  254.1 3.5 copy-start.7
  258.8 1.8 copy-start.2
  262.8 7.6 %copy-start.10 = (f32[3,512]{1,0:T(4,128)S(1)}, f32[3,512]{1,0:T(4,128)}, u32[]{:S(2)}) copy-start(f32[3,512]{1,0:T(4,128)} %param.30) | copy-start | bytes 18436
  268.2 109.3 %copy-start.4 = (bf16[1,256,2048]{2,1,0:T(8,128)(2,1)S(1)}, bf16[1,256,2048]{2,1,0:T(8,128)(2,1)}, u32[]{:S(2)}) copy-start(bf16[1,256,2048]{2,1,0:T(8,128)(2,1)} %all-gather.30.cloned.1.call-done) | copy-start | bytes 3145732
  268.2 245.7 %all-gather.20.cloned.1.call-start = ((), (), s32[]{:S(2)}) async-start(), calls=%async_computation.4 | async-start | bytes 4456448 | tf_op jit(solution)/shard_map/all_gather | solution.py:133
  269.0 306.3 %all-gather.22.cloned.1.call-start = ((), (), s32[]{:S(2)}) async-start(), calls=%async_computation.5 | async-start | bytes 2228224 | tf_op jit(solution)/shard_map/all_gather | solution.py:130
  269.7 369.9 %all-gather.28.cloned.1.call-start = ((), (), s32[]{:S(2)}) async-start(), calls=%async_computation.8 | async-start | bytes 2228224 | tf_op jit(solution)/shard_map/all_gather | solution.py:134
  270.3 381.6 %reduce-scatter.2.cloned.1.call-start = ((), (), s32[]{:S(2)}) async-start(), calls=%async_computation.9 | async-start | bytes 1572864 | tf_op jit(solution)/shard_map/reduce_scatter | solution.py:175
  318.3 79.7 %copy-start.1 = (f32[8,4,64,128]{3,0,1,2:T(8,128)S(1)}, f32[8,4,64,128]{3,0,1,2:T(8,128)}, u32[]{:S(2)}) copy-start(f32[8,4,64,128]{3,0,1,2:T(8,128)} %get-tuple-element.132) | copy-start | bytes 3145732
  377.5 20.5 %copy-start.5 = (f32[8,4,64,128]{3,0,1,2:T(8,128)S(1)}, f32[8,4,64,128]{3,0,1,2:T(8,128)}, u32[]{:S(2)}) copy-start(f32[8,4,64,128]{3,0,1,2:T(8,128)} %get-tuple-element.129) | copy-start | bytes 3145732
  379.9 18.1 %copy-start.6 = (f32[256,512]{1,0:T(8,128)}, f32[256,512]{1,0:T(8,128)S(1)}, u32[]{:S(2)}) copy-start(f32[256,512]{1,0:T(8,128)S(1)} %fusion.21) | copy-start | bytes 1572868
  380.0 259.7 %collective-permute-start = (f32[2,512]{1,0:T(2,128)S(1)}, f32[2,512]{1,0:T(2,128)S(1)}, u32[]{:S(2)}, u32[]{:S(2)}) collective-permute-start(f32[2,512]{1,0:T(2,128)S(1)} %slice.29), channel_id=1, source_target_pairs={{0,8},{8,16},{16,24},{1,9},{9,17},{17,25},{2,10},{10,18},{18,26},{... | collective-permute-start | bytes 12296 | tf_op jit(solution)/shard_map/ppermute | solution.py:27
  423.8 1.0 copy-start.8
  430.2 84.1 %copy-start.9 = (f32[1024]{0:T(1024)S(1)}, f32[1024]{0:T(1024)}, u32[]{:S(2)}) copy-start(f32[1024]{0:T(1024)} %param.29) | copy-start | bytes 12292
  514.3 125.4 %copy-start.11 = (f32[512]{0:T(512)S(1)}, f32[512]{0:T(512)}, u32[]{:S(2)}) copy-start(f32[512]{0:T(512)} %param.31) | copy-start | bytes 6148
  (1 other events, 0.8 us)
Sparse Core Ops, SparseCore 0:
  8.9 11.7 all-gather.29
  23.4 76.7 all-gather.13
  103.0 74.1 all-gather.15
  179.8 74.1 all-gather.17
  256.7 58.9 all-gather.25
  318.3 59.1 all-gather.23
  379.1 44.5 all-gather.31
  426.4 87.4 all-gather.19
  516.7 58.5 all-gather.21
  577.9 61.7 all-gather.27
  645.3 6.5 reduce-scatter.1
where the time goes:
time: 659 us; the launch traced here: 658 us
  waiting for transfers between devices  577 us (88%)
  matrix products  36.7 us (6%)
  blocking collectives  13.9 us (2%)
  between operations  13.6 us (2%)
  other arithmetic  8.04 us (1%)
    all_gather x1, waiting for transfers between devices, shards(): lax.all_gather(recurrence_output_weight, ('sp', 'fs'), axis=1, tiled=True)  81.8 us
    all_gather x1, waiting for transfers between devices, shards(): lax.all_gather(query_weight, ('sp', 'fs'), axis=0, tiled=True)  79.6 us
    all_gather x1, waiting for transfers between devices, shards(): lax.all_gather(forget_weight, ('sp', 'fs'), axis=0, tiled=True)  73.2 us
    all_gather x1, waiting for transfers between devices, shards(): lax.all_gather(value_weight, ('sp', 'fs'), axis=0, tiled=True)  72.3 us
    all_gather x1, waiting for transfers between devices, shards(): lax.all_gather(convolution_output_weight, ('sp', 'fs'), axis=1, tiled=True)  64.3 us
    all_gather x1, waiting for transfers between devices, shards(): lax.all_gather(convolution_multiplier_weight, ('sp', 'fs'), axis=0, tiled...  59.2 us
    all_gather x1, waiting for transfers between devices, shards(): lax.all_gather(convolution_gate_weight, ('sp', 'fs'), axis=0, tiled=True)  57.4 us
    all_gather x1, waiting for transfers between devices, shards(): lax.all_gather(convolution_input_weight, ('sp', 'fs'), axis=0, tiled=True)  45.3 us
  transfers between devices with their start and end apart: 12, of which 11 were waited for; matrix products, arithmetic and copies ran while one was open for 7% of the time, Pallas kernels for 0%

commit v1 on v0

--- a/solution.py
+++ b/solution.py
@@ -130,7 +130,7 @@
         lax.all_gather(convolution_gate_weight, ("sp", "fs"), axis=0, tiled=True),
         lax.all_gather(convolution_multiplier_weight, ("sp", "fs"), axis=0, tiled=True),
         lax.all_gather(convolution_input_weight, ("sp", "fs"), axis=0, tiled=True),
-        lax.all_gather(recurrence_output_weight, ("sp", "fs"), axis=1, tiled=True),
+        jnp.concatenate(lax.all_gather(recurrence_output_weight, axis_name=("sp", "fs")), axis=1),
         lax.all_gather(convolution_output_weight, ("sp", "fs"), axis=1, tiled=True),
     )
     in_weights = gathered[:6]

time: 659 us -> 646 us (0.980)
  waiting for transfers between devices: 577 us -> 559 us
    all_gather x1, waiting for transfers between devices: 81.8 us -> 58.1 us  [shards(): lax.all_gather(recurrence_output_weight, axis_name=('sp', 'fs'))]
    all_gather x1, waiting for transfers between devices: 22.1 us -> 32.8 us  [carried_in(): gathered = jax.tree.map(lambda a: lax.all_gather(a, axis), part)]
    all_gather x1, waiting for transfers between devices: 79.6 us -> 73 us  [shards(): lax.all_gather(query_weight, ('sp', 'fs'), axis=0, tiled=True)]
  transfers between devices with their start and end apart: 12 -> 12, of which waited for: 11 -> 11; matrix products, arithmetic and copies ran while one was open for 7% -> 8% of each run, Pallas kernels for 0% -> 0%
where the time goes in v1:
time: 646 us; the launch traced here: 645 us
  waiting for transfers between devices  559 us (87%)
  matrix products  35.8 us (6%)
  between operations  13.5 us (2%)
  blocking collectives  13.4 us (2%)
  local copies, waits for them, and re-layouts  10.5 us (2%)
  other arithmetic  9.54 us (1%)
    all_gather x1, waiting for transfers between devices, shards(): lax.all_gather(forget_weight, ('sp', 'fs'), axis=0, tiled=True)  79.6 us
    all_gather x1, waiting for transfers between devices, shards(): lax.all_gather(query_weight, ('sp', 'fs'), axis=0, tiled=True)  73 us
    all_gather x1, waiting for transfers between devices, shards(): lax.all_gather(value_weight, ('sp', 'fs'), axis=0, tiled=True)  72.2 us
    all_gather x1, waiting for transfers between devices, shards(): lax.all_gather(convolution_output_weight, ('sp', 'fs'), axis=1, tiled=True)  64.3 us
    all_gather x1, waiting for transfers between devices, shards(): lax.all_gather(convolution_multiplier_weight, ('sp', 'fs'), axis=0, tiled...  59.2 us
    all_gather x1, waiting for transfers between devices, shards(): lax.all_gather(recurrence_output_weight, axis_name=('sp', 'fs'))  58.1 us
    all_gather x1, waiting for transfers between devices, shards(): lax.all_gather(convolution_gate_weight, ('sp', 'fs'), axis=0, tiled=True)  52.7 us
    all_gather x1, waiting for transfers between devices, shards(): lax.all_gather(convolution_input_weight, ('sp', 'fs'), axis=0, tiled=True)  46.2 us
  transfers between devices with their start and end apart: 12, of which 11 were waited for; matrix products, arithmetic and copies ran while one was open for 8% of the time, Pallas kernels for 0%

profile of v1, /device:TPU:0, one launch (start us, length us, event | category | flops | bytes accessed | tf_op | source)
XLA Modules:
  0.0 645.4 jit_solution(3989105264493336645)
XLA Ops:
  12.2 8.5 %all-gather.29.cloned.1.call-done = bf16[1,256,2048]{2,1,0:T(8,128)(2,1)} async-done(((bf16[1,128,2048]{2,1,0:T(8,128)(2,1)}), bf16[1,256,2048]{2,1,0:T(8,128)(2,1)}) %all-gather.29.cloned.1.call-update) | async-done | bytes 1048592 | tf_op jit(solution)/shard_map/all_gather | solution.py:139
  20.7 79.6 %all-gather.17.cloned.1.call-done = bf16[2048,1024]{1,0:T(8,128)(2,1)} async-done(((bf16[128,1024]{1,0:T(8,128)(2,1)}), bf16[2048,1024]{1,0:T(8,128)(2,1)}) %all-gather.17.cloned.1.call-update) | async-done | bytes 4194320 | tf_op jit(solution)/shard_map/all_gather | solution.py:128
  100.2 3.8 fusion.14
  104.3 73.0 %all-gather.15.cloned.1.call-done = bf16[2048,1024]{1,0:T(8,128)(2,1)} async-done(((bf16[128,1024]{1,0:T(8,128)(2,1)}), bf16[2048,1024]{1,0:T(8,128)(2,1)}) %all-gather.15.cloned.1.call-update) | async-done | bytes 4194320 | tf_op jit(solution)/shard_map/all_gather | solution.py:127
  177.2 3.4 fusion.17
  181.8 72.2 %all-gather.19.cloned.1.call-done = bf16[2048,1024]{1,0:T(8,128)(2,1)} async-done(((bf16[128,1024]{1,0:T(8,128)(2,1)}), bf16[2048,1024]{1,0:T(8,128)(2,1)}) %all-gather.19.cloned.1.call-update) | async-done | bytes 4194320 | tf_op jit(solution)/shard_map/all_gather | solution.py:129
  254.1 3.4 fusion.18
  262.7 4.6 while.26
  269.5 46.2 %all-gather.25.cloned.1.call-done = bf16[2048,512]{1,0:T(8,128)(2,1)} async-done(((bf16[128,512]{1,0:T(8,128)(2,1)}), bf16[2048,512]{1,0:T(8,128)(2,1)}) %all-gather.25.cloned.1.call-update) | async-done | bytes 2097168 | tf_op jit(solution)/shard_map/all_gather | solution.py:132
  315.7 2.6 fusion.22
  318.3 59.2 %all-gather.23.cloned.1.call-done = bf16[2048,512]{1,0:T(8,128)(2,1)} async-done(((bf16[128,512]{1,0:T(8,128)(2,1)}), bf16[2048,512]{1,0:T(8,128)(2,1)}) %all-gather.23.cloned.1.call-update) | async-done | bytes 2097168 | tf_op jit(solution)/shard_map/all_gather | solution.py:131
  377.5 2.3 fusion.21
  379.9 3.4 collective-permute-start
  383.2 13.4 %all-gather.1 = f32[32,128]{1,0:T(8,128)S(1)} all-gather(f32[8,128]{1,0:T(8,128)S(1)} %exp.41), channel_id=3, replica_groups=mesh['sp'=4,'fs'=4,'tp'=2] {'sp'}, dimensions={0}, use_global_device_ids=true | all-gather | bytes 20480 | tf_op jit(solution)/shard_map/all_gather | solution.py:13
  396.6 58.1 %all-gather.33.cloned.1.call-done = bf16[16384,128]{1,0:T(8,128)(2,1)} async-done(((bf16[1024,128]{1,0:T(8,128)(2,1)}), bf16[16384,128]{1,0:T(8,128)(2,1)}) %all-gather.33.cloned.1.call-update) | async-done | bytes 4194320 | tf_op jit(solution)/shard_map/all_gather | solution.py:133
  454.7 6.5 %copy.56 = bf16[1024,16,128]{0,2,1:T(8,128)(2,1)} copy(bf16[1024,16,128]{2,0,1:T(8,128)(2,1)} %bitcast.128) | data formatting | bytes 8388608 | tf_op jit(solution)/shard_map/reshape | solution.py:133
  461.2 4.1 convolution_select_fusion
  467.8 32.8 %all-gather.31.cloned.1.call-done = f32[32,128,128]{2,1,0:T(8,128)} async-done(((f32[8,128,128]{2,1,0:T(8,128)}), f32[32,128,128]{2,1,0:T(8,128)}) %all-gather.31.cloned.1.call-update) | async-done | bytes 2097168 | tf_op jit(solution)/shard_map/all_gather | solution.py:13
  502.0 4.4 multiply_reduce_fusion
  507.2 2.7 fusion.46
  509.8 52.7 %all-gather.21.cloned.1.call-done = bf16[2048,512]{1,0:T(8,128)(2,1)} async-done(((bf16[128,512]{1,0:T(8,128)(2,1)}), bf16[2048,512]{1,0:T(8,128)(2,1)}) %all-gather.21.cloned.1.call-update) | async-done | bytes 2097168 | tf_op jit(solution)/shard_map/all_gather | solution.py:130
  562.6 64.3 %all-gather.27.cloned.1.call-done = bf16[512,2048]{1,0:T(8,128)(2,1)} async-done(((bf16[512,128]{1,0:T(8,128)(2,1)}), bf16[512,2048]{1,0:T(8,128)(2,1)}) %all-gather.27.cloned.1.call-update) | async-done | bytes 2097168 | tf_op jit(solution)/shard_map/all_gather | solution.py:134
  626.9 5.3 fusion
  632.2 6.7 %reduce-scatter.2.cloned.1.call-done = bf16[128,2048]{1,0:T(8,128)(2,1)} async-done(((bf16[256,2048]{1,0:T(8,128)(2,1)}), bf16[128,2048]{1,0:T(8,128)(2,1)}) %reduce-scatter.2.cloned.1.call-update) | async-done | bytes 524304 | tf_op jit(solution)/shard_map/reduce_scatter | solution.py:175
  (82 shorter events, 23.3 us)
Async XLA Ops:
  6.5 14.1 %all-gather.29.cloned.1.call-start = ((), (), s32[]{:S(2)}) async-start(), calls=%async_computation.9 | async-start | bytes 1572864 | tf_op jit(solution)/shard_map/all_gather | solution.py:139
  7.3 93.0 %all-gather.17.cloned.1.call-start = ((), (), s32[]{:S(2)}) async-start(), calls=%async_computation.2 | async-start | bytes 4456448 | tf_op jit(solution)/shard_map/all_gather | solution.py:128
  8.0 169.2 %all-gather.15.cloned.1.call-start = ((), (), s32[]{:S(2)}) async-start(), calls=%async_computation.1 | async-start | bytes 4456448 | tf_op jit(solution)/shard_map/all_gather | solution.py:127
  8.7 245.3 %all-gather.19.cloned.1.call-start = ((), (), s32[]{:S(2)}) async-start(), calls=%async_computation.3 | async-start | bytes 4456448 | tf_op jit(solution)/shard_map/all_gather | solution.py:129
  9.3 306.4 %all-gather.25.cloned.1.call-start = ((), (), s32[]{:S(2)}) async-start(), calls=%async_computation.6 | async-start | bytes 2228224 | tf_op jit(solution)/shard_map/all_gather | solution.py:132
  9.9 367.6 %all-gather.23.cloned.1.call-start = ((), (), s32[]{:S(2)}) async-start(), calls=%async_computation.5 | async-start | bytes 2228224 | tf_op jit(solution)/shard_map/all_gather | solution.py:131
  10.5 444.2 %all-gather.33.cloned.1.call-start = ((), (), s32[]{:S(2)}) async-start(), calls=%async_computation.11 | async-start | bytes 4456448 | tf_op jit(solution)/shard_map/all_gather | solution.py:133
  11.2 489.3 %all-gather.31.cloned.1.call-start = ((), (), s32[]{:S(2)}) async-start(), calls=%async_computation.10 | async-start | bytes 2621440 | tf_op jit(solution)/shard_map/all_gather | solution.py:13
  104.1 73.2 %copy-start.4 = (bf16[1,256,2048]{2,1,0:T(8,128)(2,1)S(1)}, bf16[1,256,2048]{2,1,0:T(8,128)(2,1)}, u32[]{:S(2)}) copy-start(bf16[1,256,2048]{2,1,0:T(8,128)(2,1)} %all-gather.29.cloned.1.call-done) | copy-start | bytes 3145732
  257.5 1.2 copy-start.7
  258.3 2.2 copy-start.2
  262.7 6.9 %copy-start.8 = (f32[3,512]{1,0:T(4,128)S(1)}, f32[3,512]{1,0:T(4,128)}, u32[]{:S(2)}) copy-start(f32[3,512]{1,0:T(4,128)} %param.30) | copy-start | bytes 18436
  267.3 0.8 copy-start
  268.1 109.4 %copy-start.5 = (bf16[1,256,2048]{2,1,0:T(8,128)(2,1)S(1)}, bf16[1,256,2048]{2,1,0:T(8,128)(2,1)}, u32[]{:S(2)}) copy-start(bf16[1,256,2048]{2,1,0:T(8,128)(2,1)} %all-gather.29.cloned.1.call-done) | copy-start | bytes 3145732
  268.1 294.4 %all-gather.21.cloned.1.call-start = ((), (), s32[]{:S(2)}) async-start(), calls=%async_computation.4 | async-start | bytes 2228224 | tf_op jit(solution)/shard_map/all_gather | solution.py:130
  268.9 358.0 %all-gather.27.cloned.1.call-start = ((), (), s32[]{:S(2)}) async-start(), calls=%async_computation.7 | async-start | bytes 2228224 | tf_op jit(solution)/shard_map/all_gather | solution.py:134
  269.5 369.4 %reduce-scatter.2.cloned.1.call-start = ((), (), s32[]{:S(2)}) async-start(), calls=%async_computation.8 | async-start | bytes 1572864 | tf_op jit(solution)/shard_map/reduce_scatter | solution.py:175
  379.9 247.0 %collective-permute-start = (f32[2,512]{1,0:T(2,128)S(1)}, f32[2,512]{1,0:T(2,128)S(1)}, u32[]{:S(2)}, u32[]{:S(2)}) collective-permute-start(f32[2,512]{1,0:T(2,128)S(1)} %slice.29), channel_id=1, source_target_pairs={{0,8},{8,16},{16,24},{1,9},{9,17},{17,25},{2,10},{10,18},{18,26},{... | collective-permute-start | bytes 12296 | tf_op jit(solution)/shard_map/ppermute | solution.py:27
  454.7 6.5 %copy-start.1 = (f32[8,4,64,128]{3,0,1,2:T(8,128)S(1)}, f32[8,4,64,128]{3,0,1,2:T(8,128)}, u32[]{:S(2)}) copy-start(f32[8,4,64,128]{3,0,1,2:T(8,128)} %get-tuple-element.137) | copy-start | bytes 3145732
  500.6 1.4 copy-start.6
  502.0 4.4 copy-start.9
  502.0 5.1 copy-start.3
  507.2 119.7 %copy-start.10 = (f32[512]{0:T(512)S(1)}, f32[512]{0:T(512)}, u32[]{:S(2)}) copy-start(f32[512]{0:T(512)} %param.31) | copy-start | bytes 6148
Sparse Core Ops, SparseCore 0:
  8.9 11.7 all-gather.28
  23.4 76.7 all-gather.16
  103.0 74.1 all-gather.14
  179.8 74.1 all-gather.18
  256.7 58.9 all-gather.24
  318.3 59.1 all-gather.22
  380.3 74.3 all-gather.32
  456.3 44.2 all-gather.30
  503.3 59.1 all-gather.20
  565.1 61.7 all-gather.26
  632.3 6.5 reduce-scatter.1
